TPU v7x, 32 devices: a whole 2x2x4 slice. The times are simulated.
32 devices in a mesh: ep: 8 (over z, x), tp: 4 (over y, core).
Axes of the slice: x: 2, y: 2, z: 4, core: 2. Of those that a mesh axis runs over, the one named last changes fastest.
Arguments:
- mixer_rows: bfloat16 [1024, 2048], P('ep'), may hold values from -40 to 40
- mixer_gain: float32 [2048], replicated, may hold values from 0.1 to 1.9
- inner_weight: bfloat16 [2048, 1024], P(None, 'tp'), may hold values from -0.125 to 0.125
- gate_in_weight: bfloat16 [2048, 1024], P(None, 'tp'), may hold values from -0.125 to 0.125
- gate_out_weight: bfloat16 [2048, 1024], P(None, 'tp'), may hold values from -0.125 to 0.125
- conv_taps: float32 [3, 1024], P(None, 'tp'), may hold values from -3.5 to 3.5
- mixer_out_weight: bfloat16 [1024, 2048], P('tp'), may hold values from -0.1875 to 0.1875
- routed_rows: bfloat16 [2048, 2048], P('ep'), may hold values from -40 to 40
- routed_gain: float32 [2048], replicated, may hold values from 0.1 to 1.9
- route_ids: int32 [2048, 2], P('ep'), may hold values from 0 to 7, all different within a row; in each aligned block of 256 rows (0 to 255, 256 to 511, ...) at most 128 rows name the same one
- route_weights: float32 [2048, 2], P('ep'), may hold values from 0.25 to 1
- expert_gate: bfloat16 [8, 2048, 2048], P('ep', None, 'tp'), may hold values from -0.125 to 0.125
- expert_up: bfloat16 [8, 2048, 2048], P('ep', None, 'tp'), may hold values from -0.125 to 0.125
- expert_down: bfloat16 [8, 2048, 2048], P('ep', 'tp'), may hold values from -0.125 to 0.125
Outputs:
- mixer_output: bfloat16 [1024, 2048], P('ep')
- routed_output: bfloat16 [2048, 2048], P('ep')
Inputs may be any that keep to these rules, and one draw needn't show every extreme that they name: `route_ids`: within each aligned block of 256 tokens, no expert is named by more than 128 choices, a bound that some block reaches; a token's 2 experts differ.
All inputs are finite; a program needn't handle non-finite values.
Results may differ from a plain program's by a relative error of at most 0.019.
Values may be sent and summed in bfloat16 or wider, within the bound.
A program may use at most 64 MiB of HBM per device.

v0:
```python
import jax
import jax.numpy as jnp
from jax import lax
from jax.sharding import PartitionSpec as P


def shifted(value, axis, steps):
    count = lax.axis_size(axis)
    initial, last = (max(0, -steps), min(count, count - steps))
    return lax.ppermute(value, axis, [(source, source + steps) for source in range(initial, last)])


def rms_scale(row_block, gain_row):
    values = row_block.astype(jnp.float32)
    scaled = values * lax.rsqrt(jnp.mean(values * values, axis=-1, keepdims=True) + 1e-06)
    return (scaled * gain_row).astype(jnp.bfloat16)


def on_device(
    mixer_rows,
    mixer_gain,
    inner_weight,
    gate_in_weight,
    gate_out_weight,
    conv_taps,
    mixer_out_weight,
    routed_rows,
    routed_gain,
    route_ids,
    route_weights,
    expert_gate,
    expert_up,
    expert_down,
):
    normed = rms_scale(mixer_rows, mixer_gain)
    inner_proj = jnp.dot(normed, inner_weight, preferred_element_type=jnp.float32)
    gate_in = jnp.dot(normed, gate_in_weight, preferred_element_type=jnp.float32)
    conv_input = (gate_in * inner_proj).astype(jnp.bfloat16)
    gate_out = jnp.dot(normed, gate_out_weight, preferred_element_type=jnp.float32)
    tap_total = conv_taps.shape[0]
    rim_rows = tap_total - 1
    earlier_rows = shifted(conv_input[conv_input.shape[0] - rim_rows :], "ep", 1)
    extended = jnp.concatenate([earlier_rows, conv_input], axis=0).astype(jnp.float32)
    length = conv_input.shape[0]
    conv_out = jnp.zeros(conv_input.shape, jnp.float32)
    for tap_index in range(tap_total):
        conv_out = conv_out + conv_taps[tap_index] * extended[tap_index : tap_index + length]
    gated_conv = (gate_out * conv_out).astype(jnp.bfloat16)
    mixer_terms = jnp.dot(gated_conv, mixer_out_weight, preferred_element_type=jnp.float32)
    routed_normed = rms_scale(routed_rows, routed_gain)
    experts = lax.axis_size("ep")
    groups = lax.axis_size("tp")
    column = lax.axis_index("tp")
    tok_count, pick_count = route_ids.shape
    model_width = routed_rows.shape[1]
    capacity = 2 * tok_count * pick_count // experts
    share_rows = capacity // groups
    flat_ids = route_ids.reshape(-1)
    onehot = (flat_ids[:, None] == jnp.arange(experts, dtype=jnp.int32)[None, :]).astype(jnp.int32)
    slot_rank = jnp.sum((jnp.cumsum(onehot, axis=0) - onehot) * onehot, axis=1)
    slot_number = slot_rank * experts + flat_ids
    owners = jnp.arange(tok_count * pick_count, dtype=jnp.int32) // pick_count
    matches = slot_number[None, :] == jnp.arange(capacity * experts, dtype=jnp.int32)[:, None]
    token_table = jnp.where(
        jnp.any(matches, axis=1), jnp.sum(jnp.where(matches, owners[None, :], 0), axis=1), tok_count
    )
    padded_rows = jnp.concatenate(
        [routed_normed, jnp.zeros((1, model_width), jnp.bfloat16)], axis=0
    )
    table_share = lax.dynamic_slice_in_dim(
        token_table.reshape(capacity, experts), column * share_rows, share_rows, 0
    )
    outgoing = jnp.take(padded_rows, table_share.reshape(-1), axis=0).reshape(
        share_rows, experts, model_width
    )
    arrived = lax.all_to_all(outgoing, "ep", split_axis=1, concat_axis=1, tiled=True)
    incoming = lax.all_gather(arrived, "tp", axis=0, tiled=True)
    slot_rows = incoming.reshape(capacity * experts, model_width)
    gate_act = jnp.dot(slot_rows, expert_gate[0], preferred_element_type=jnp.float32)
    up_act = jnp.dot(slot_rows, expert_up[0], preferred_element_type=jnp.float32)
    hidden = (jax.nn.silu(gate_act) * up_act).astype(jnp.bfloat16)
    summed = lax.psum_scatter(
        jnp.dot(hidden, expert_down[0], preferred_element_type=jnp.float32).astype(jnp.bfloat16),
        "tp",
        scatter_dimension=0,
        tiled=True,
    )
    returned = lax.all_to_all(
        summed.reshape(share_rows, experts, model_width),
        "ep",
        split_axis=1,
        concat_axis=1,
        tiled=True,
    )
    flat_back = jnp.concatenate(
        [
            returned.reshape(share_rows * experts, model_width),
            jnp.zeros((1, model_width), jnp.bfloat16),
        ],
        axis=0,
    )
    local_slot = jnp.where(
        slot_rank // share_rows == column,
        (slot_rank - column * share_rows) * experts + flat_ids,
        share_rows * experts,
    )
    contrib = (
        jnp.take(flat_back, local_slot, axis=0).astype(jnp.float32)
        * route_weights.reshape(-1)[:, None]
    )
    routed_terms = jnp.sum(contrib.reshape(tok_count, pick_count, model_width), axis=1)
    mixer_total, routed_total = (
        lax.psum(mixer_terms.astype(jnp.bfloat16), "tp").astype(jnp.float32),
        lax.psum(routed_terms.astype(jnp.bfloat16), "tp").astype(jnp.float32),
    )
    return (mixer_total.astype(jnp.bfloat16), routed_total.astype(jnp.bfloat16))


def solution(mesh):
    return jax.shard_map(
        on_device,
        mesh=mesh,
        in_specs=(
            P("ep", None),
            P(),
            P(None, "tp"),
            P(None, "tp"),
            P(None, "tp"),
            P(None, "tp"),
            P("tp", None),
            P("ep", None),
            P(),
            P("ep", None),
            P("ep", None),
            P("ep", None, "tp"),
            P("ep", None, "tp"),
            P("ep", "tp", None),
        ),
        out_specs=(P("ep", None), P("ep", None)),
        check_vma=False,
    )
```

profile of v0, /device:TPU:0, one launch (start us, length us, event | category | flops | bytes accessed | tf_op | source)
XLA Modules:
  0.0 255.2 jit_solution(8111063935972421025)
XLA Ops:
  8.5 1.1 reduce-window.6
  10.9 1.5 fusion.4
  13.6 2.3 gather_fusion
  15.9 2.4 copy_select_fusion
  18.4 32.8 %all_to_all.10 = bf16[32,8,2048]{2,0,1:T(8,128)(2,1)S(1)} all-to-all(bf16[32,8,2048]{2,0,1:T(8,128)(2,1)S(1)} %copy_select_fusion), channel_id=1, replica_groups=mesh['ep'=8,'tp'=4] {'ep'}, dimensions={1} | all-to-all | bytes 2097152 | tf_op jit(solution)/shard_map/all_to_all | solution.py:76
  51.2 1.5 copy.77
  52.8 33.6 %all-gather.2.cloned.1.call-done = bf16[128,8,2048]{2,1,0:T(8,128)(2,1)} async-done(((bf16[32,8,2048]{2,1,0:T(8,128)(2,1)}), bf16[128,8,2048]{2,1,0:T(8,128)(2,1)}) %all-gather.2.cloned.1.call-update) | async-done | bytes 4194320 | tf_op jit(solution)/shard_map/all_gather | solution.py:77
  86.4 6.6 %fusion.2 = f32[1024,512]{1,0:T(8,128)} fusion(bf16[128,8,2048]{2,1,0:T(8,128)(2,1)} %all-gather.2.cloned.1.call-done, bf16[1,2048,512]{2,1,0:T(8,128)(2,1)} %param.25), kind=kOutput, calls=%fused_computation.4 | convolution fusion | flops 2147483648 | bytes 8388608 | tf_op jit(solution)/shard_map/dot_general | solution.py:79
  93.0 10.0 %convolution_convert_fusion = bf16[1024,2048]{1,0:T(8,128)(2,1)} fusion(bf16[1,512,2048]{2,1,0:T(8,128)(2,1)S(1)} %copy-done, f32[1024,512]{1,0:T(8,128)} %fusion.2, bf16[1,2048,512]{2,1,0:T(8,128)(2,1)} %param.26, bf16[128,8,2048]{2,1,0:T(8,128)(2,1)} %all-gather.2.cloned.1.call-done), kind=kOutput, calls=%fused_computation.8 | convolution fusion | flops 4300210176 | bytes 14680064 | tf_op jit(solution)/shard_map/dot_general | solution.py:83
  103.0 1.0 copy-done.2
  104.2 43.5 %reduce-scatter.2.cloned.1.call-done = bf16[256,2048]{1,0:T(8,128)(2,1)} async-done(((bf16[1024,2048]{1,0:T(8,128)(2,1)}), bf16[256,2048]{1,0:T(8,128)(2,1)}) %reduce-scatter.2.cloned.1.call-update) | async-done | bytes 1048592 | tf_op jit(solution)/shard_map/reduce_scatter | solution.py:82
  147.7 2.8 %copy.78 = bf16[32,8,2048]{2,0,1:T(8,128)(2,1)} copy(bf16[32,8,2048]{2,1,0:T(8,128)(2,1)} %bitcast.47) | data formatting | bytes 2097152 | tf_op jit(solution)/shard_map/reshape | solution.py:89
  150.5 5.5 %all-to-all-start.1 = ((bf16[32,8,2048]{2,0,1:T(8,128)(2,1)}), bf16[32,8,2048]{2,0,1:T(8,128)(2,1)S(1)}, u32[]{:S(2)}, u32[]{:S(2)}) async-start(bf16[32,8,2048]{2,0,1:T(8,128)(2,1)} %copy.78), calls=%async_computation.2 | async-start | bytes 2097152 | tf_op jit(solution)/shard_map/all_to_all | solution.py:88
  156.1 1.7 fusion.40
  157.9 1.8 fusion.16
  159.7 4.1 %collective-permute-start = (bf16[2,256]{1,0:T(2,128)(2,1)S(1)}, bf16[2,256]{1,0:T(2,128)(2,1)S(1)}, u32[]{:S(2)}, u32[]{:S(2)}) collective-permute-start(bf16[2,256]{1,0:T(2,128)(2,1)S(1)} %slice.40), channel_id=1, source_target_pairs={{0,4},{4,8},{8,12},{12,16},{16,20},{20,24},{24,28},{1,5},{5,9},{9,... | collective-permute-start | bytes 3080 | tf_op jit(solution)/shard_map/ppermute | solution.py:10
  164.9 3.3 %convolution_convert_fusion.1 = bf16[128,2048]{1,0:T(8,128)(2,1)} fusion(bf16[256,2048]{1,0:T(8,128)(2,1)} %param.20, bf16[2048,256]{1,0:T(8,128)(2,1)} %param.18, f32[130,256]{1,0:T(8,128)S(1)} %maximum_convert_fusion, f32[256]{0:T(256)S(1)} %bitcast.51, f32[256]{0:T(256)S(1)} %bitcast.52, f32[256]{0:T(256)S(1)} %bitcast.50, bf16[128,2048]{1,0:T(8,128)(2,1)} %param.14, ...), kind=kOutput, calls=%fused_computation.11 | convolution fusion | flops 269975552 | bytes 3550720 | tf_op jit(solution)/shard_map/dot_general | solution.py:49
  168.2 13.5 %all-to-all-done.1 = bf16[32,8,2048]{2,0,1:T(8,128)(2,1)S(1)} async-done(((bf16[32,8,2048]{2,0,1:T(8,128)(2,1)}), bf16[32,8,2048]{2,0,1:T(8,128)(2,1)S(1)}, u32[]{:S(2)}, u32[]{:S(2)}) %all-to-all-start.1) | async-done | bytes 1048608 | tf_op jit(solution)/shard_map/all_to_all | solution.py:88
  182.4 3.3 %gather_fusion.1 = bf16[512,2048]{1,0:T(8,128)(2,1)} fusion(bf16[257,2048]{1,0:T(8,128)(2,1)S(1)} %concatenate.11, s32[1024]{0:T(1024)S(1)} %pad_clamp_fusion), kind=kCustom, calls=%fused_computation.1 | custom fusion | bytes 4196352 | tf_op jit(solution)/shard_map/jit(_take)/gather | solution.py:108
  185.7 4.4 %gather.15 = bf16[256,2,2048]{2,1,0:T(2,128)(2,1)} reshape(bf16[512,2048]{1,0:T(8,128)(2,1)} %gather_fusion.1) | data formatting | bytes 4194304 | tf_op jit(solution)/shard_map/jit(_take)/gather | solution.py:108
  190.1 10.8 %multiply_reduce_fusion = bf16[256,2048]{1,0:T(8,128)(2,1)} fusion(bf16[256,2,2048]{2,1,0:T(2,128)(2,1)} %gather.15, pred[256,2]{1,0:T(8,128)(4,1)S(1)} %copy.74, f32[256,2]{1,0:T(8,128)S(1)} %copy.81), kind=kLoop, calls=%fused_computation.6 | loop fusion | flops 3670016 | bytes 3148288 | tf_op jit(solution)/shard_map/reduce_sum | solution.py:111
  201.0 43.5 %all-reduce.5.cloned.1.call-done = (bf16[128,2048]{1,0:T(8,128)(2,1)}, bf16[256,2048]{1,0:T(8,128)(2,1)}) async-done(((bf16[128,2048]{1,0:T(8,128)(2,1)}, bf16[256,2048]{1,0:T(8,128)(2,1)}), (bf16[128,2048]{1,0:T(8,128)(2,1)}, bf16[256,2048]{1,0:T(8,128)(2,1)})) %all-reduce.5.cloned.1.call-update) | async-done | bytes 1572880 | tf_op jit(solution)/shard_map/psum | solution.py:113
  244.5 1.9 copy.87
  246.4 2.3 copy.88
  (56 shorter events, 5.7 us)
Async XLA Ops:
  7.2 85.8 %copy-start = (bf16[1,512,2048]{2,1,0:T(8,128)(2,1)S(1)}, bf16[1,512,2048]{2,1,0:T(8,128)(2,1)}, u32[]{:S(2)}) copy-start(bf16[1,512,2048]{2,1,0:T(8,128)(2,1)} %param.27) | copy-start | bytes 6291460
  7.2 5.3 %copy-start.1 = (bf16[256,2048]{1,0:T(8,128)(2,1)S(1)}, bf16[256,2048]{1,0:T(8,128)(2,1)}, u32[]{:S(2)}) copy-start(bf16[256,2048]{1,0:T(8,128)(2,1)} %param.21) | copy-start | bytes 3145732
  7.2 79.2 %all-gather.2.cloned.1.call-start = ((), (), s32[]{:S(2)}) async-start(), calls=%async_computation.3 | async-start | bytes 5242880 | tf_op jit(solution)/shard_map/all_gather | solution.py:77
  52.8 95.0 %reduce-scatter.2.cloned.1.call-start = ((), (), s32[]{:S(2)}) async-start(), calls=%async_computation.4 | async-start | bytes 5242880 | tf_op jit(solution)/shard_map/reduce_scatter | solution.py:82
  103.0 1.0 copy-start.2
  147.7 8.4 %copy-start.3 = (f32[2048]{0:T(1024)S(1)}, f32[2048]{0:T(1024)}, u32[]{:S(2)}) copy-start(f32[2048]{0:T(1024)} %param.15) | copy-start | bytes 24580
  150.5 31.2 %all-to-all-start.1 = ((bf16[32,8,2048]{2,0,1:T(8,128)(2,1)}), bf16[32,8,2048]{2,0,1:T(8,128)(2,1)S(1)}, u32[]{:S(2)}, u32[]{:S(2)}) async-start(bf16[32,8,2048]{2,0,1:T(8,128)(2,1)} %copy.78), calls=%async_computation.2 | async-start | bytes 2097152 | tf_op jit(solution)/shard_map/all_to_all | solution.py:88
  156.0 8.1 %copy-start.4 = (s32[256,2]{0,1:T(2,128)S(1)}, s32[256,2]{0,1:T(2,128)}, u32[]{:S(2)}) copy-start(s32[256,2]{0,1:T(2,128)} %param.23) | copy-start | bytes 6148
  156.0 8.1 %copy-start.5 = (f32[3,256]{1,0:T(4,128)S(1)}, f32[3,256]{1,0:T(4,128)}, u32[]{:S(2)}) copy-start(f32[3,256]{1,0:T(4,128)} %param.19) | copy-start | bytes 9220
  156.0 88.4 %all-reduce.5.cloned.1.call-start = ((), (), s32[]{:S(2)}) async-start(), calls=%async_computation.5 | async-start | bytes 3145728 | tf_op jit(solution)/shard_map/psum | solution.py:113
  156.1 8.3 %copy-start.6 = (f32[256,2]{0,1:T(2,128)S(1)}, f32[256,2]{0,1:T(2,128)}, u32[]{:S(2)}) copy-start(f32[256,2]{0,1:T(2,128)} %param.24) | copy-start | bytes 6148
  159.7 5.2 %collective-permute-start = (bf16[2,256]{1,0:T(2,128)(2,1)S(1)}, bf16[2,256]{1,0:T(2,128)(2,1)S(1)}, u32[]{:S(2)}, u32[]{:S(2)}) collective-permute-start(bf16[2,256]{1,0:T(2,128)(2,1)S(1)} %slice.40), channel_id=1, source_target_pairs={{0,4},{4,8},{8,12},{12,16},{16,20},{20,24},{24,28},{1,5},{5,9},{9,... | collective-permute-start | bytes 3080 | tf_op jit(solution)/shard_map/ppermute | solution.py:10
Sparse Core Ops, SparseCore 0:
  52.9 33.4 all-gather.1
  103.1 44.5 reduce-scatter.1
  201.1 43.3 all-reduce.4
where the time goes:
time: 256 us; the launch traced here: 255 us
  waiting for transfers between devices  134 us (52%)
  blocking collectives  32.8 us (13%)
  matrix products  23.4 us (9%)
  local copies, waits for them, and re-layouts  22.8 us (9%)
  other arithmetic  18 us (7%)
  between operations  14 us (5%)
  starting transfers between devices  9.73 us (4%)
    reduce_scatter x1, waiting for transfers between devices, on_device(): lax.psum_scatter(jnp.dot(hidden, expert_down[0], preferred_element_type=j...  43.5 us
    psum x1, waiting for transfers between devices, on_device(): lax.psum(mixer_terms.astype(jnp.bfloat16), 'tp').astype(jnp.float32)  43.5 us
    all_gather x1, waiting for transfers between devices, on_device(): incoming = lax.all_gather(arrived, 'tp', axis=0, tiled=True)  33.6 us
    all_to_all x1, blocking collectives, on_device(): lax.all_to_all(outgoing, 'ep', split_axis=1, concat_axis=1, tiled=True)  32.8 us
    all_to_all x1, waiting for transfers between devices, on_device(): lax.all_to_all(summed.reshape(share_rows, experts, model_width), 'ep', sp...  13.5 us
    reduce_sum x1, other arithmetic, on_device(): jnp.sum(contrib.reshape(tok_count, pick_count, model_width), axis=1)  10.8 us
    dot_general x1, matrix products, on_device(): jnp.dot(hidden, expert_down[0], preferred_element_type=jnp.float32)  9.96 us
    gather x2, local copies, waits for them, and re-layouts, on_device(): jnp.take(flat_back, local_slot, axis=0).astype(jnp.float32)  7.75 us
  transfers between devices with their start and end apart: 5, of which 5 were waited for; matrix products, arithmetic and copies ran while one was open for 3% of the time, Pallas kernels for 0%

commit v1 on v0

v1 whole, which is shorter than its diff:
```python
import jax
import jax.numpy as jnp
from jax import lax
from jax.experimental import pallas as pl
from jax.experimental.pallas import tpu as pltpu
from jax.sharding import PartitionSpec as P

F32, BF16, I32 = jnp.float32, jnp.bfloat16, jnp.int32
CORES = 2


def rms(values):
    return lax.rsqrt(jnp.mean(values * values, axis=-1, keepdims=True) + 1e-06)


def dot(a, b):
    return jnp.dot(a, b, preferred_element_type=F32)


def make_kernel(experts, groups, tok, picks, width, cap, steps, per, mrows, taps_n, chan):
    high = groups // CORES
    slab = width // groups
    rows = per * cap

    def kernel(
        mixer_rows, mixer_gain, inner_h, gate_in_h, gate_out_h, taps, mixer_out_h,
        routed_rows, routed_gain, ids, weights, gate_h, up_h, down_h,
        out_m, out_r,
        w_inner, w_gin, w_gout, w_mout, w_gate, w_up, w_down,
        disp, slots, part, r1, s2, r2, t3, ret,
        rim, rim_in, m_part, m_r1, m_s2, m_r2,
        w_sem, own_sem,
        d1_s, d1_r, y_s, y_r, b_s, b_r, e_s, e_r, g_s, g_r, ret_s, ret_r,
        rim_s, rim_r, ay_s, ay_r, ab_s, ab_r,
    ):
        me = lax.axis_index("ep")
        t = lax.axis_index("tp")
        yy, cc = t // CORES, t % CORES
        mate = yy * CORES + (1 - cc)
        my_chunk, my_j = me // per, me % per
        sent = []

        def send(src, dst, ssem, rsem, where):
            copy = pltpu.make_async_remote_copy(
                src_ref=src, dst_ref=dst, send_sem=ssem, recv_sem=rsem,
                device_id=where, device_id_type=pl.DeviceIdType.MESH,
            )
            copy.start()
            sent.append(copy)

        def arrive(dst, ssem, rsem):
            pltpu.make_async_remote_copy(
                src_ref=dst, dst_ref=dst, send_sem=ssem, recv_sem=rsem,
                device_id={"tp": mate}, device_id_type=pl.DeviceIdType.MESH,
            ).wait_recv()

        def up_to(dy):
            return lax.rem(yy + dy, high)

        def down_to(dy):
            return lax.rem(yy + high - dy, high)

        loads = []
        for place, (src, dst) in enumerate(
            (
                (inner_h, w_inner), (gate_in_h, w_gin), (gate_out_h, w_gout), (mixer_out_h, w_mout),
                (gate_h, w_gate), (up_h, w_up), (down_h, w_down),
            )
        ):
            copy = pltpu.make_async_copy(src, dst, w_sem.at[place])
            copy.start()
            loads.append(copy)

        barrier = pltpu.get_barrier_semaphore()
        for d in range(1, experts):
            pl.semaphore_signal(
                barrier, inc=1, device_id={"ep": lax.rem(me + d, experts)},
                device_id_type=pl.DeviceIdType.MESH,
            )
        for dy in range(1, high):
            pl.semaphore_signal(
                barrier, inc=1, device_id={"tp": up_to(dy) * CORES + cc},
                device_id_type=pl.DeviceIdType.MESH,
            )
        pl.semaphore_signal(
            barrier, inc=1, device_id={"tp": mate}, device_id_type=pl.DeviceIdType.MESH
        )

        lane = lax.broadcasted_iota(I32, (tok, 128), 1)
        hits = [lane == ids[:, k : k + 1] for k in range(picks)]
        named = sum(h.astype(F32) for h in hits)
        before = (
            lax.broadcasted_iota(I32, (tok, tok), 0) > lax.broadcasted_iota(I32, (tok, tok), 1)
        ).astype(F32).astype(BF16)
        earlier = dot(before, named.astype(BF16))
        slot_lane = lax.broadcasted_iota(I32, (tok, experts * cap), 1)
        pick_map = jnp.zeros((tok, experts * cap), F32)
        sum_map = jnp.zeros((tok, experts * cap), F32)
        for k in range(picks):
            rank = jnp.sum(jnp.where(hits[k], earlier, 0.0), axis=1, keepdims=True).astype(I32)
            at = slot_lane == (ids[:, k : k + 1] * cap + rank)
            pick_map = pick_map + jnp.where(at, 1.0, 0.0)
            sum_map = sum_map + jnp.where(at, weights[:, k : k + 1], 0.0)
        pick_map, sum_map = pick_map.astype(BF16), sum_map.astype(BF16)

        my_cols = pl.ds(pl.multiple_of(t * slab, slab), slab)
        scale = rms(routed_rows[...].astype(F32))
        normed = ((routed_rows[:, my_cols].astype(F32) * scale) * routed_gain[:, my_cols]).astype(BF16)
        disp[...] = (
            lax.dot_general(pick_map, normed, (((0,), (0,)), ((), ())), preferred_element_type=F32)
            .astype(BF16)
            .reshape(experts, cap, slab)
        )
        pl.semaphore_wait(barrier, experts - 1 + high - 1 + 1)

        for i in range(steps):
            chunk = lax.rem(my_chunk + steps - i, steps)
            for j in range(per if i else per - 1):
                jj = j if i else lax.rem(my_j + j + 1, per)
                dest = chunk * per + jj
                send(
                    disp.at[dest], slots.at[t, i, my_j], d1_s.at[i, jj], d1_r.at[i, my_j], {"ep": dest}
                )
        own = pltpu.make_async_copy(disp.at[me], slots.at[t, 0, my_j], own_sem.at[0])
        own.start()

        def stage_a(i):
            for j in range(per if i else per - 1):
                jj = j if i else lax.rem(my_j + j + 1, per)
                arrive(slots.at[t, i, jj], d1_s.at[i, jj], d1_r.at[i, jj])
            if i == 0:
                own.wait()
            for dy in range(1, high):
                send(
                    slots.at[t, i], slots.at[t, i], y_s.at[i, dy - 1], y_r.at[i, dy - 1],
                    {"tp": up_to(dy) * CORES + cc},
                )
            send(slots.at[t, i], slots.at[t, i], b_s.at[i, 0], b_r.at[i, 0], {"tp": mate})

        def stage_b(i):
            for dy in range(1, high):
                block = slots.at[down_to(dy) * CORES + cc, i]
                arrive(block, y_s.at[i, dy - 1], y_r.at[i, dy - 1])
                send(block, block, b_s.at[i, dy], b_r.at[i, dy], {"tp": mate})

        def stage_c(i):
            for dy in range(high):
                arrive(
                    slots.at[down_to(dy) * CORES + (1 - cc), i], b_s.at[i, dy], b_r.at[i, dy]
                )
            if i == 0:
                for copy in loads[4:]:
                    copy.wait()
            x = jnp.concatenate([slots[q, i].reshape(rows, slab) for q in range(groups)], axis=1)
            gate, up = dot(x, w_gate[...]), dot(x, w_up[...])
            hidden = (gate / (1.0 + jnp.exp(-gate)) * up).astype(BF16)
            for q in range(groups):
                part[i, q % CORES, q // CORES] = dot(
                    hidden, w_down[:, q * slab : (q + 1) * slab]
                ).astype(BF16)
            send(part.at[i, 1 - cc], r1.at[i], e_s.at[i], e_r.at[i], {"tp": mate})

        def pair_sum(i, part_i, r1_i, s2_i, r2_i):
            arrive(r1_i, e_s.at[i], e_r.at[i])
            for y in range(high):
                s2_i[y] = (part_i[cc, y].astype(F32) + r1_i[y].astype(F32)).astype(BF16)
            for dy in range(1, high):
                send(
                    s2_i.at[up_to(dy)], r2_i.at[dy - 1], g_s.at[i, dy - 1], g_r.at[i, dy - 1],
                    {"tp": up_to(dy) * CORES + cc},
                )

        def chip_sum(i, s2_i, r2_i):
            total = s2_i[yy].astype(F32)
            for dy in range(1, high):
                arrive(r2_i.at[dy - 1], g_s.at[i, dy - 1], g_r.at[i, dy - 1])
                total = total + r2_i[dy - 1].astype(F32)
            return total.astype(BF16)

        def stage_e(i):
            pair_sum(i, part.at[i], r1.at[i], s2.at[i], r2.at[i])

        def stage_g(i):
            t3[i] = chip_sum(i, s2.at[i], r2.at[i]).reshape(per, cap, slab)
            chunk = lax.rem(my_chunk + i, steps)
            for j in range(per if i else per - 1):
                jj = j if i else lax.rem(my_j + j + 1, per)
                dest = chunk * per + jj
                send(t3.at[i, jj], ret.at[me], ret_s.at[i, jj], ret_r.at[me], {"ep": dest})
            if i == 0:
                ret[me] = t3[0, my_j]

        def spread(which, out, value):
            out[:, my_cols] = value
            window = out.at[:, my_cols]
            for dy in range(1, high):
                send(
                    window, window, ay_s.at[which, dy - 1], ay_r.at[which, dy - 1],
                    {"tp": up_to(dy) * CORES + cc},
                )
            send(window, window, ab_s.at[which, 0], ab_r.at[which, 0], {"tp": mate})

        def window_of(out, group):
            return out.at[:, pl.ds(pl.multiple_of(group * slab, slab), slab)]

        def spread_on(which, out):
            for dy in range(1, high):
                window = window_of(out, down_to(dy) * CORES + cc)
                arrive(window, ay_s.at[which, dy - 1], ay_r.at[which, dy - 1])
                send(window, window, ab_s.at[which, dy], ab_r.at[which, dy], {"tp": mate})

        def spread_end(which, out):
            for dy in range(high):
                arrive(
                    window_of(out, down_to(dy) * CORES + (1 - cc)),
                    ab_s.at[which, dy], ab_r.at[which, dy],
                )

        for copy in loads[:4]:
            copy.wait()
        mixed = mixer_rows[...].astype(F32)
        mixed = ((mixed * rms(mixed)) * mixer_gain[...]).astype(BF16)
        conv_input = (dot(mixed, w_gin[...]) * dot(mixed, w_inner[...])).astype(BF16)
        edge = rim.shape[0]
        rim[...] = conv_input[mrows - edge :]
        send(rim, rim_in, rim_s.at[0], rim_r.at[0], {"ep": lax.rem(me + 1, experts)})
        gate_out = dot(mixed, w_gout[...])
        stage_a(0)
        arrive(rim_in, rim_s.at[0], rim_r.at[0])
        first = jnp.where(me == 0, 0.0, rim_in[...].astype(F32))
        extended = jnp.concatenate([first, conv_input.astype(F32)], axis=0)
        conv = jnp.zeros((mrows, chan), F32)
        for k in range(taps_n):
            start = edge - (taps_n - 1) + k
            conv = conv + taps[k : k + 1, :] * extended[start : start + mrows]
        gated = (gate_out * conv).astype(BF16)
        for q in range(groups):
            m_part[q % CORES, q // CORES] = dot(gated, w_mout[:, q * slab : (q + 1) * slab]).astype(BF16)
        send(m_part.at[1 - cc], m_r1, e_s.at[steps], e_r.at[steps], {"tp": mate})

        for s in range(1, steps + 4):
            if s < steps:
                stage_a(s)
            if s - 1 < steps:
                stage_b(s - 1)
            if s == 1:
                pair_sum(steps, m_part, m_r1, m_s2, m_r2)
            if 0 <= s - 2 < steps:
                stage_e(s - 2)
            if s == 2:
                spread(0, out_m, chip_sum(steps, m_s2, m_r2))
            if s == 3:
                spread_on(0, out_m)
            if s - 1 < steps:
                stage_c(s - 1)
            if 0 <= s - 3 < steps:
                stage_g(s - 3)

        for d in range(1, experts):
            e = lax.rem(me + d, experts)
            arrive(ret.at[e], ret_s.at[0, 0], ret_r.at[e])
        spread(1, out_r, dot(sum_map, ret[...].reshape(experts * cap, slab)).astype(BF16))
        spread_on(1, out_r)
        spread_end(0, out_m)
        spread_end(1, out_r)
        for copy in sent:
            copy.wait_send()

    edge = 16 * -(-(taps_n - 1) // 16)
    dma = pltpu.SemaphoreType.DMA
    far = max(1, high - 1)
    hid_scratch = lambda shape, kind=BF16: pltpu.VMEM(shape, kind)
    v = hid_scratch

    def scratch(hid):
        return [
            v((width, chan)), v((width, chan)), v((width, chan)), v((chan, width)),
            v((width, hid)), v((width, hid)), v((hid, width)),
            v((experts, cap, slab)), v((groups, steps, per, cap, slab)),
            v((steps, CORES, high, rows, slab)), v((steps, high, rows, slab)),
            v((steps, high, rows, slab)), v((steps, far, rows, slab)),
            v((steps, per, cap, slab)), v((experts, cap, slab)),
            v((edge, chan)), v((edge, chan)),
            v((CORES, high, mrows, slab)), v((high, mrows, slab)), v((high, mrows, slab)),
            v((far, mrows, slab)),
            dma((7,)), dma((1,)),
            dma((steps, per)), dma((steps, per)), dma((steps, far)), dma((steps, far)),
            dma((steps, high)), dma((steps, high)), dma((steps + 1,)), dma((steps + 1,)),
            dma((steps + 1, far)), dma((steps + 1, far)), dma((steps, per)), dma((experts,)),
            dma((1,)), dma((1,)), dma((2, far)), dma((2, far)), dma((2, high)), dma((2, high)),
        ]

    return kernel, scratch


def on_device(
    mixer_rows, mixer_gain, inner_weight, gate_in_weight, gate_out_weight, conv_taps,
    mixer_out_weight, routed_rows, routed_gain, route_ids, route_weights,
    expert_gate, expert_up, expert_down,
):
    experts, groups = lax.axis_size("ep"), lax.axis_size("tp")
    tok, picks = route_ids.shape
    width = routed_rows.shape[1]
    cap = 2 * tok * picks // experts
    per = max(1, min(experts, tok // cap))
    steps = experts // per
    mrows = mixer_rows.shape[0]
    taps_n, chan = conv_taps.shape
    kernel, scratch = make_kernel(
        experts, groups, tok, picks, width, cap, steps, per, mrows, taps_n, chan
    )
    near, far = pl.BlockSpec(memory_space=pltpu.VMEM), pl.BlockSpec(memory_space=pl.ANY)
    return pl.pallas_call(
        kernel,
        out_shape=(
            jax.ShapeDtypeStruct(mixer_rows.shape, BF16),
            jax.ShapeDtypeStruct(routed_rows.shape, BF16),
        ),
        in_specs=[near, near, far, far, far, near, far, near, near, near, near, far, far, far],
        out_specs=(near, near),
        scratch_shapes=scratch(expert_gate.shape[2]),
        compiler_params=pltpu.CompilerParams(
            collective_id=0, has_side_effects=True, vmem_limit_bytes=60 * 1024 * 1024
        ),
        name="mixer_and_experts",
    )(
        mixer_rows, mixer_gain[None, :], inner_weight, gate_in_weight, gate_out_weight, conv_taps,
        mixer_out_weight, routed_rows, routed_gain[None, :], route_ids, route_weights,
        expert_gate[0], expert_up[0], expert_down[0],
    )


def solution(mesh):
    return jax.shard_map(
        on_device,
        mesh=mesh,
        in_specs=(
            P("ep", None), P(), P(None, "tp"), P(None, "tp"), P(None, "tp"), P(None, "tp"),
            P("tp", None), P("ep", None), P(), P("ep", None), P("ep", None),
            P("ep", None, "tp"), P("ep", None, "tp"), P("ep", "tp", None),
        ),
        out_specs=(P("ep", None), P("ep", None)),
        check_vma=False,
    )
```

time: 256 us -> 102 us (0.40)
  the two profiles are of different devices: /device:TPU:0 before, /device:TPU:7 now
where the time goes in v1:
time: 102 us; the launch traced here: 101 us
  Pallas kernels  93.6 us (92%)
  local copies, waits for them, and re-layouts  7.14 us (7%)
    pallas_call x1, Pallas kernels, on_device(): pl.pallas_call(kernel, out_shape=(jax.ShapeDtypeStruct(mixer_rows.shape,...  93.6 us
    unnamed x4, local copies, waits for them, and re-layouts  7.14 us

profile of v1, /device:TPU:7, one launch (start us, length us, event | category | flops | bytes accessed | tf_op | source)
XLA Modules:
  0.0 101.4 jit_solution(10056984408341700316)
XLA Ops:
  0.6 1.5 %copy.16.ids = s32[256,2]{1,0:T(8,128)} copy(s32[256,2]{0,1:T(2,128)} %param.23) | data formatting | bytes 4096 | tf_op args[9]
  2.1 1.5 %copy.17.weights = f32[256,2]{1,0:T(8,128)} copy(f32[256,2]{0,1:T(2,128)} %param.24) | data formatting | bytes 4096 | tf_op args[10]
  3.6 93.6 %mixer_and_experts.1 = (bf16[128,2048]{1,0:T(8,128)(2,1)}, bf16[256,2048]{1,0:T(8,128)(2,1)}) custom-call(bf16[128,2048]{1,0:T(8,128)(2,1)} %mixer_rows.1, f32[1,2048]{1,0:T(1,128)} %bitcast.8, bf16[2048,256]{1,0:T(8,128)(2,1)} %inner_h.1, bf16[2048,256]{1,0:T(8,128)(2,1)} %gate_in_h.1, bf16[2048,256]{1,0:T(8,128)(2,1)} %gate_out_h.1, f32[3,256]{1,0:T(4,128)} %taps.1, ...), custom_call_target="tpu_custom_call" | custom-call | tf_op jit(solution)/shard_map/mixer_and_experts/pallas_call | solution.py:313
  97.2 1.9 %copy.20 = bf16[128,2048]{1,0:T(8,128)(2,1)} copy(bf16[128,2048]{1,0:T(8,128)(2,1)} %get-tuple-element.4) | data formatting | bytes 1048576
  99.1 2.3 %copy.21 = bf16[256,2048]{1,0:T(8,128)(2,1)} copy(bf16[256,2048]{1,0:T(8,128)(2,1)} %get-tuple-element.5) | data formatting | bytes 2097152

commit v2 on v1

--- a/solution.py
+++ b/solution.py
@@ -19,6 +19,7 @@
 
 def make_kernel(experts, groups, tok, picks, width, cap, steps, per, mrows, taps_n, chan):
     high = groups // CORES
+    whole = min(2, steps)
     slab = width // groups
     rows = per * cap
 
@@ -86,58 +87,83 @@
             barrier, inc=1, device_id={"tp": mate}, device_id_type=pl.DeviceIdType.MESH
         )
 
-        lane = lax.broadcasted_iota(I32, (tok, 128), 1)
-        hits = [lane == ids[:, k : k + 1] for k in range(picks)]
+        row = lax.broadcasted_iota(I32, (128, tok), 0)
+        hits = [row == ids[k : k + 1, :] for k in range(picks)]
         named = sum(h.astype(F32) for h in hits)
         before = (
-            lax.broadcasted_iota(I32, (tok, tok), 0) > lax.broadcasted_iota(I32, (tok, tok), 1)
+            lax.broadcasted_iota(I32, (tok, tok), 0) < lax.broadcasted_iota(I32, (tok, tok), 1)
         ).astype(F32).astype(BF16)
-        earlier = dot(before, named.astype(BF16))
-        slot_lane = lax.broadcasted_iota(I32, (tok, experts * cap), 1)
-        pick_map = jnp.zeros((tok, experts * cap), F32)
-        sum_map = jnp.zeros((tok, experts * cap), F32)
+        earlier = dot(named.astype(BF16), before)
+        slot_row = lax.broadcasted_iota(I32, (experts * cap, tok), 0)
+        pick_map = jnp.zeros((experts * cap, tok), F32)
+        sum_map = jnp.zeros((experts * cap, tok), F32)
         for k in range(picks):
-            rank = jnp.sum(jnp.where(hits[k], earlier, 0.0), axis=1, keepdims=True).astype(I32)
-            at = slot_lane == (ids[:, k : k + 1] * cap + rank)
+            rank = jnp.sum(jnp.where(hits[k], earlier, 0.0), axis=0, keepdims=True).astype(I32)
+            at = slot_row == (ids[k : k + 1, :] * cap + rank)
             pick_map = pick_map + jnp.where(at, 1.0, 0.0)
-            sum_map = sum_map + jnp.where(at, weights[:, k : k + 1], 0.0)
+            sum_map = sum_map + jnp.where(at, weights[k : k + 1, :], 0.0)
         pick_map, sum_map = pick_map.astype(BF16), sum_map.astype(BF16)
 
         my_cols = pl.ds(pl.multiple_of(t * slab, slab), slab)
         scale = rms(routed_rows[...].astype(F32))
-        normed = ((routed_rows[:, my_cols].astype(F32) * scale) * routed_gain[:, my_cols]).astype(BF16)
-        disp[...] = (
-            lax.dot_general(pick_map, normed, (((0,), (0,)), ((), ())), preferred_element_type=F32)
-            .astype(BF16)
-            .reshape(experts, cap, slab)
-        )
+        for y in range(high):
+            cols = pl.ds(pl.multiple_of((y * CORES + cc) * slab, slab), slab)
+            normed = ((routed_rows[:, cols].astype(F32) * scale) * routed_gain[:, cols]).astype(BF16)
+            disp[y] = dot(pick_map, normed).astype(BF16).reshape(experts, cap, slab)
         pl.semaphore_wait(barrier, experts - 1 + high - 1 + 1)
 
+        def others(i):
+            return [j if i else lax.rem(my_j + j + 1, per) for j in range(per if i else per - 1)]
+
+        def partner(i):
+            chunk = my_chunk
+            for bit in (1 << n for n in range(i.bit_length())):
+                if i & bit:
+                    chunk = chunk + bit - 2 * bit * lax.rem(chunk // bit, 2)
+            return chunk
+
+        def slabs(i):
+            return range(high if i < whole else 1)
+
         for i in range(steps):
-            chunk = lax.rem(my_chunk + steps - i, steps)
-            for j in range(per if i else per - 1):
-                jj = j if i else lax.rem(my_j + j + 1, per)
-                dest = chunk * per + jj
-                send(
-                    disp.at[dest], slots.at[t, i, my_j], d1_s.at[i, jj], d1_r.at[i, my_j], {"ep": dest}
-                )
-        own = pltpu.make_async_copy(disp.at[me], slots.at[t, 0, my_j], own_sem.at[0])
-        own.start()
+            for jj in others(i):
+                dest = partner(i) * per + jj
+                for dy in slabs(i):
+                    y = down_to(dy)
+                    send(
+                        disp.at[y, dest], slots.at[y * CORES + cc, i, my_j],
+                        d1_s.at[i, jj, dy], d1_r.at[i, my_j, dy], {"ep": dest},
+                    )
+        own = []
+        for y in range(high):
+            copy = pltpu.make_async_copy(
+                disp.at[y, me], slots.at[y * CORES + cc, 0, my_j], own_sem.at[y]
+            )
+            copy.start()
+            own.append(copy)
 
         def stage_a(i):
-            for j in range(per if i else per - 1):
-                jj = j if i else lax.rem(my_j + j + 1, per)
-                arrive(slots.at[t, i, jj], d1_s.at[i, jj], d1_r.at[i, jj])
+            for jj in others(i):
+                for dy in slabs(i):
+                    arrive(
+                        slots.at[down_to(dy) * CORES + cc, i, jj], d1_s.at[i, jj, dy], d1_r.at[i, jj, dy]
+                    )
             if i == 0:
-                own.wait()
-            for dy in range(1, high):
-                send(
-                    slots.at[t, i], slots.at[t, i], y_s.at[i, dy - 1], y_r.at[i, dy - 1],
-                    {"tp": up_to(dy) * CORES + cc},
-                )
-            send(slots.at[t, i], slots.at[t, i], b_s.at[i, 0], b_r.at[i, 0], {"tp": mate})
+                for copy in own:
+                    copy.wait()
+            if i >= whole:
+                for dy in range(1, high):
+                    send(
+                        slots.at[t, i], slots.at[t, i], y_s.at[i, dy - 1], y_r.at[i, dy - 1],
+                        {"tp": up_to(dy) * CORES + cc},
+                    )
+            for dy in slabs(i):
+                block = slots.at[down_to(dy) * CORES + cc, i]
+                send(block, block, b_s.at[i, dy], b_r.at[i, dy], {"tp": mate})
 
         def stage_b(i):
+            if i < whole:
+                return
             for dy in range(1, high):
                 block = slots.at[down_to(dy) * CORES + cc, i]
                 arrive(block, y_s.at[i, dy - 1], y_r.at[i, dy - 1])
@@ -182,10 +208,8 @@
 
         def stage_g(i):
             t3[i] = chip_sum(i, s2.at[i], r2.at[i]).reshape(per, cap, slab)
-            chunk = lax.rem(my_chunk + i, steps)
-            for j in range(per if i else per - 1):
-                jj = j if i else lax.rem(my_j + j + 1, per)
-                dest = chunk * per + jj
+            for jj in others(i):
+                dest = partner(i) * per + jj
                 send(t3.at[i, jj], ret.at[me], ret_s.at[i, jj], ret_r.at[me], {"ep": dest})
             if i == 0:
                 ret[me] = t3[0, my_j]
@@ -238,28 +262,30 @@
             m_part[q % CORES, q // CORES] = dot(gated, w_mout[:, q * slab : (q + 1) * slab]).astype(BF16)
         send(m_part.at[1 - cc], m_r1, e_s.at[steps], e_r.at[steps], {"tp": mate})
 
-        for s in range(1, steps + 4):
-            if s < steps:
-                stage_a(s)
-            if s - 1 < steps:
-                stage_b(s - 1)
+        for s in range(steps):
+            stage_b(s)
+            stage_c(s)
+            if s + 1 < steps:
+                stage_a(s + 1)
+            if s == 0:
+                pair_sum(steps, m_part, m_r1, m_s2, m_r2)
+            stage_e(s)
             if s == 1:
-                pair_sum(steps, m_part, m_r1, m_s2, m_r2)
-            if 0 <= s - 2 < steps:
-                stage_e(s - 2)
+                spread(0, out_m, chip_sum(steps, m_s2, m_r2))
             if s == 2:
-                spread(0, out_m, chip_sum(steps, m_s2, m_r2))
-            if s == 3:
                 spread_on(0, out_m)
-            if s - 1 < steps:
-                stage_c(s - 1)
-            if 0 <= s - 3 < steps:
-                stage_g(s - 3)
+            if s >= 1:
+                stage_g(s - 1)
+        stage_g(steps - 1)
 
         for d in range(1, experts):
             e = lax.rem(me + d, experts)
             arrive(ret.at[e], ret_s.at[0, 0], ret_r.at[e])
-        spread(1, out_r, dot(sum_map, ret[...].reshape(experts * cap, slab)).astype(BF16))
+        summed = lax.dot_general(
+            sum_map, ret[...].reshape(experts * cap, slab), (((0,), (0,)), ((), ())),
+            preferred_element_type=F32,
+        )
+        spread(1, out_r, summed.astype(BF16))
         spread_on(1, out_r)
         spread_end(0, out_m)
         spread_end(1, out_r)
@@ -276,15 +302,15 @@
         return [
             v((width, chan)), v((width, chan)), v((width, chan)), v((chan, width)),
             v((width, hid)), v((width, hid)), v((hid, width)),
-            v((experts, cap, slab)), v((groups, steps, per, cap, slab)),
+            v((high, experts, cap, slab)), v((groups, steps, per, cap, slab)),
             v((steps, CORES, high, rows, slab)), v((steps, high, rows, slab)),
             v((steps, high, rows, slab)), v((steps, far, rows, slab)),
             v((steps, per, cap, slab)), v((experts, cap, slab)),
             v((edge, chan)), v((edge, chan)),
             v((CORES, high, mrows, slab)), v((high, mrows, slab)), v((high, mrows, slab)),
             v((far, mrows, slab)),
-            dma((7,)), dma((1,)),
-            dma((steps, per)), dma((steps, per)), dma((steps, far)), dma((steps, far)),
+            dma((7,)), dma((high,)),
+            dma((steps, per, high)), dma((steps, per, high)), dma((steps, far)), dma((steps, far)),
             dma((steps, high)), dma((steps, high)), dma((steps + 1,)), dma((steps + 1,)),
             dma((steps + 1, far)), dma((steps + 1, far)), dma((steps, per)), dma((experts,)),
             dma((1,)), dma((1,)), dma((2, far)), dma((2, far)), dma((2, high)), dma((2, high)),
@@ -325,7 +351,7 @@
         name="mixer_and_experts",
     )(
         mixer_rows, mixer_gain[None, :], inner_weight, gate_in_weight, gate_out_weight, conv_taps,
-        mixer_out_weight, routed_rows, routed_gain[None, :], route_ids, route_weights,
+        mixer_out_weight, routed_rows, routed_gain[None, :], route_ids.T, route_weights.T,
         expert_gate[0], expert_up[0], expert_down[0],
     )
 

time: 102 us -> 107 us (1.049)
  the two profiles are of different devices: /device:TPU:7 before, /device:TPU:23 now
where the time goes in v2:
time: 107 us
  Pallas kernels  102 us (95%)
  local copies, waits for them, and re-layouts  4.18 us (4%)
    pallas_call x1, Pallas kernels, on_device(): pl.pallas_call(kernel, out_shape=(jax.ShapeDtypeStruct(mixer_rows.shape,...  102 us
    unnamed x2, local copies, waits for them, and re-layouts  4.18 us

profile of v2, /device:TPU:23, one launch (start us, length us, event | category | flops | bytes accessed | tf_op | source)
XLA Modules:
  0.0 106.5 jit_solution(1402571144830423505)
XLA Ops:
  0.6 101.7 %mixer_and_experts.1 = (bf16[128,2048]{1,0:T(8,128)(2,1)}, bf16[256,2048]{1,0:T(8,128)(2,1)}) custom-call(bf16[128,2048]{1,0:T(8,128)(2,1)} %mixer_rows.1, f32[1,2048]{1,0:T(1,128)} %bitcast.10, bf16[2048,256]{1,0:T(8,128)(2,1)} %inner_h.1, bf16[2048,256]{1,0:T(8,128)(2,1)} %gate_in_h.1, bf16[2048,256]{1,0:T(8,128)(2,1)} %gate_out_h.1, f32[3,256]{1,0:T(4,128)} %taps.1, ...), custom_call_target="tpu_custom_call" | custom-call | tf_op jit(solution)/shard_map/mixer_and_experts/pallas_call | solution.py:339
  102.3 1.9 %copy.18 = bf16[128,2048]{1,0:T(8,128)(2,1)} copy(bf16[128,2048]{1,0:T(8,128)(2,1)} %get-tuple-element.4) | data formatting | bytes 1048576
  104.2 2.3 %copy.19 = bf16[256,2048]{1,0:T(8,128)(2,1)} copy(bf16[256,2048]{1,0:T(8,128)(2,1)} %get-tuple-element.5) | data formatting | bytes 2097152

commit v3 on v2

--- a/solution.py
+++ b/solution.py
@@ -19,7 +19,9 @@
 
 def make_kernel(experts, groups, tok, picks, width, cap, steps, per, mrows, taps_n, chan):
     high = groups // CORES
-    whole = min(2, steps)
+    whole = 1
+    half = steps // 2
+    order = list(range(half, steps)) + list(range(half - 1, -1, -1))
     slab = width // groups
     rows = per * cap
 
@@ -125,7 +127,7 @@
         def slabs(i):
             return range(high if i < whole else 1)
 
-        for i in range(steps):
+        for i in order:
             for jj in others(i):
                 dest = partner(i) * per + jj
                 for dy in slabs(i):
@@ -174,9 +176,6 @@
                 arrive(
                     slots.at[down_to(dy) * CORES + (1 - cc), i], b_s.at[i, dy], b_r.at[i, dy]
                 )
-            if i == 0:
-                for copy in loads[4:]:
-                    copy.wait()
             x = jnp.concatenate([slots[q, i].reshape(rows, slab) for q in range(groups)], axis=1)
             gate, up = dot(x, w_gate[...]), dot(x, w_up[...])
             hidden = (gate / (1.0 + jnp.exp(-gate)) * up).astype(BF16)
@@ -249,7 +248,7 @@
         rim[...] = conv_input[mrows - edge :]
         send(rim, rim_in, rim_s.at[0], rim_r.at[0], {"ep": lax.rem(me + 1, experts)})
         gate_out = dot(mixed, w_gout[...])
-        stage_a(0)
+        stage_a(order[0])
         arrive(rim_in, rim_s.at[0], rim_r.at[0])
         first = jnp.where(me == 0, 0.0, rim_in[...].astype(F32))
         extended = jnp.concatenate([first, conv_input.astype(F32)], axis=0)
@@ -262,21 +261,23 @@
             m_part[q % CORES, q // CORES] = dot(gated, w_mout[:, q * slab : (q + 1) * slab]).astype(BF16)
         send(m_part.at[1 - cc], m_r1, e_s.at[steps], e_r.at[steps], {"tp": mate})
 
+        for copy in loads[4:]:
+            copy.wait()
         for s in range(steps):
-            stage_b(s)
-            stage_c(s)
+            stage_b(order[s])
+            stage_c(order[s])
             if s + 1 < steps:
-                stage_a(s + 1)
+                stage_a(order[s + 1])
             if s == 0:
                 pair_sum(steps, m_part, m_r1, m_s2, m_r2)
-            stage_e(s)
+            stage_e(order[s])
             if s == 1:
                 spread(0, out_m, chip_sum(steps, m_s2, m_r2))
             if s == 2:
                 spread_on(0, out_m)
             if s >= 1:
-                stage_g(s - 1)
-        stage_g(steps - 1)
+                stage_g(order[s - 1])
+        stage_g(order[steps - 1])
 
         for d in range(1, experts):
             e = lax.rem(me + d, experts)
@@ -295,8 +296,7 @@
     edge = 16 * -(-(taps_n - 1) // 16)
     dma = pltpu.SemaphoreType.DMA
     far = max(1, high - 1)
-    hid_scratch = lambda shape, kind=BF16: pltpu.VMEM(shape, kind)
-    v = hid_scratch
+    v = lambda shape: pltpu.VMEM(shape, BF16)
 
     def scratch(hid):
         return [

time: 107 us -> 97.1 us (0.907)
  the two profiles are of different devices: /device:TPU:23 before, /device:TPU:0 now
where the time goes in v3:
time: 97.1 us; the launch traced here: 96.9 us
  Pallas kernels  92 us (95%)
  local copies, waits for them, and re-layouts  4.18 us (4%)
    pallas_call x1, Pallas kernels, on_device(): pl.pallas_call(kernel, out_shape=(jax.ShapeDtypeStruct(mixer_rows.shape,...  92 us
    unnamed x2, local copies, waits for them, and re-layouts  4.18 us

profile of v3, /device:TPU:0, one launch (start us, length us, event | category | flops | bytes accessed | tf_op | source)
XLA Modules:
  0.0 96.9 jit_solution(18305409999321363038)
XLA Ops:
  0.6 92.0 %mixer_and_experts.1 = (bf16[128,2048]{1,0:T(8,128)(2,1)}, bf16[256,2048]{1,0:T(8,128)(2,1)}) custom-call(bf16[128,2048]{1,0:T(8,128)(2,1)} %mixer_rows.1, f32[1,2048]{1,0:T(1,128)} %bitcast.10, bf16[2048,256]{1,0:T(8,128)(2,1)} %inner_h.1, bf16[2048,256]{1,0:T(8,128)(2,1)} %gate_in_h.1, bf16[2048,256]{1,0:T(8,128)(2,1)} %gate_out_h.1, f32[3,256]{1,0:T(4,128)} %taps.1, ...), custom_call_target="tpu_custom_call" | custom-call | tf_op jit(solution)/shard_map/mixer_and_experts/pallas_call | solution.py:339
  92.7 1.9 %copy.18 = bf16[128,2048]{1,0:T(8,128)(2,1)} copy(bf16[128,2048]{1,0:T(8,128)(2,1)} %get-tuple-element.4) | data formatting | bytes 1048576
  94.6 2.3 %copy.19 = bf16[256,2048]{1,0:T(8,128)(2,1)} copy(bf16[256,2048]{1,0:T(8,128)(2,1)} %get-tuple-element.5) | data formatting | bytes 2097152
